TPU v7x, 32 devices: a whole 2x2x4 slice. The times are simulated.
32 devices in a mesh: kv: 8 (over z, x), tp: 4 (over y, core).
Axes of the slice: x: 2, y: 2, z: 4, core: 2. Of those that a mesh axis runs over, the one named last changes fastest.
Arguments:
- hidden_rows: bfloat16 [28, 4096], P(None, ('kv', 'tp')), may hold values from -6 to 6
- first_gain: float32 [4096], P('kv'), may hold values from 0.1 to 1.9
- first_gate: bfloat16 [4096, 11264], P('kv', 'tp'), may hold values from -0.125 to 0.125
- first_up: bfloat16 [4096, 11264], P('kv', 'tp'), may hold values from -0.125 to 0.125
- first_down: bfloat16 [11264, 4096], P('tp', 'kv'), may hold values from -0.078125 to 0.078125
- mix_gain: float32 [4096], P('kv'), may hold values from 0.1 to 1.9
- query_weight: bfloat16 [4096, 2048], P('kv', 'tp'), may hold values from -0.09375 to 0.09375
- key_weight: bfloat16 [4096, 2048], P('kv', 'tp'), may hold values from -0.09375 to 0.09375
- value_weight: bfloat16 [4096, 2048], P('kv', 'tp'), may hold values from -0.09375 to 0.09375
- forget_weight: bfloat16 [4096, 16], P('kv'), may hold values from -0.09375 to 0.09375
- forget_bias: float32 [16], replicated, may hold values from -8 to 2
- out_weight: bfloat16 [2048, 4096], P('tp', 'kv'), may hold values from -0.5 to 0.5
- second_gain: float32 [4096], P('kv'), may hold values from 0.1 to 1.9
- second_gate: bfloat16 [4096, 11264], P('kv', 'tp'), may hold values from -0.125 to 0.125
- second_up: bfloat16 [4096, 11264], P('kv', 'tp'), may hold values from -0.125 to 0.125
- second_down: bfloat16 [11264, 4096], P('tp', 'kv'), may hold values from -0.078125 to 0.078125
- cache_keys: bfloat16 [28, 2048, 2048], P(None, 'kv', 'tp'), may hold values from -48 to 48
- cache_values: bfloat16 [28, 2048, 2048], P(None, 'kv', 'tp'), may hold values from -6 to 6
- cache_gates: float32 [28, 16, 2048], P(None, 'tp', 'kv'), may hold values from -1 to 0
- lengths: int32 [28], replicated, may hold values from 1 to 2048, 16384 in all
Outputs:
- out_rows: bfloat16 [28, 4096], P(None, ('kv', 'tp'))
Inputs may be any that keep to these rules, and one draw needn't show every extreme that they name: Sequence b uses cache positions 0 to lengths[b] - 1; some sequence uses all 2048.
All inputs are finite; a program needn't handle non-finite values.
Results may differ from a plain program's by a relative error of at most 0.014.
Values may be sent and summed in bfloat16 or wider, within the bound.
No kernel may reach another device: no remote copies, remote signals or barrier semaphores. Data moves between devices by JAX's collectives and lax.ppermute only.
A program may use at most 128 MiB of HBM per device.

v0:
```python
import jax
import jax.numpy as jnp
from jax import lax
from jax.sharding import PartitionSpec as P

D = 4096
HEAD_DIM = 128
EPS = 1e-06
FLOOR = -1e30


def entering(x, axis, combine, identity):
    devices, mine = (lax.axis_size(axis), lax.axis_index(axis))
    everything = lax.all_gather(x, axis)
    start = jnp.broadcast_to(jnp.asarray(identity, x.dtype), x.shape)

    def lap(k, before):
        reached = k < mine
        new = combine(before, everything[k])
        return jnp.where(reached, new, before)

    return lax.fori_loop(0, devices, lap, start)


def joined(value, axis, join):
    pieces = jax.tree.map(lambda part: lax.all_gather(part, axis), value)
    head = jax.tree.map(lambda part: part[0], pieces)
    tail = jax.tree.map(lambda part: part[1:], pieces)
    total, _ = lax.scan(lambda total, share: (join(total, share), None), head, tail)
    return total


def widen(shard):
    return lax.all_gather(shard, "tp", axis=1, tiled=True)


def scaled_rows(block, gain):
    block32 = block.astype(jnp.float32)
    scaled = (block32 * gain).astype(jnp.bfloat16)
    squares = jnp.sum(block32 * block32, axis=1, keepdims=True)
    return (scaled, squares)


def feed_forward(block, gain, w_gate, w_up, w_down):
    scaled, squares = scaled_rows(block, gain)
    gate = jnp.dot(scaled, w_gate, preferred_element_type=jnp.float32)
    up_act = jnp.dot(scaled, w_up, preferred_element_type=jnp.float32)
    gate, up_act, squares = lax.psum((gate, up_act, squares), "kv")
    rscale = lax.rsqrt(squares / D + EPS)
    hidden = (jax.nn.silu(gate * rscale) * (up_act * rscale)).astype(jnp.bfloat16)
    return jnp.dot(hidden, w_down, preferred_element_type=jnp.float32)


def join_parts(first, second):
    top_a, mass_a, summed_a = first
    top_b, mass_b, summed_b = second
    peak = jnp.maximum(top_a, top_b)
    part_a = jnp.exp(top_a - peak)
    part_b = jnp.exp(top_b - peak)
    return (
        peak,
        mass_a * part_a + mass_b * part_b,
        summed_a * part_a[:, :, None] + summed_b * part_b[:, :, None],
    )


def attention(
    block,
    gain,
    query_weight,
    key_weight,
    value_weight,
    forget_weight,
    forget_bias,
    out_weight,
    cache_keys,
    cache_values,
    cache_gates,
    lengths,
):
    scaled, squares = scaled_rows(block, gain)
    seqs = block.shape[0]
    heads_dev = query_weight.shape[1] // HEAD_DIM
    span = cache_keys.shape[1]
    places = lax.axis_index("kv") * span + jnp.arange(span, dtype=jnp.int32)
    live = places[None, None, :] < lengths[:, None, None]
    kept = jnp.where(live, cache_gates, 0.0)
    running = jnp.cumsum(kept, axis=2)
    local_total = running[:, :, -1:]
    lower = entering(local_total, "kv", jnp.add, jnp.zeros_like(local_total))
    part_query = jnp.dot(scaled, query_weight, preferred_element_type=jnp.float32)
    part_key = jnp.dot(scaled, key_weight, preferred_element_type=jnp.float32)
    part_value = jnp.dot(scaled, value_weight, preferred_element_type=jnp.float32)
    part_logit = jnp.dot(scaled, forget_weight, preferred_element_type=jnp.float32)
    part_query, part_key, part_value, part_logit, squares, grand = lax.psum(
        (part_query, part_key, part_value, part_logit, squares, local_total), "kv"
    )
    rscale = lax.rsqrt(squares / D + EPS)
    query = (part_query * rscale).astype(jnp.bfloat16).reshape(seqs, heads_dev, HEAD_DIM)
    fresh_key = (part_key * rscale).astype(jnp.bfloat16).reshape(seqs, heads_dev, HEAD_DIM)
    fresh_value = (part_value * rscale).astype(jnp.bfloat16).reshape(seqs, heads_dev, HEAD_DIM)
    first_head = lax.axis_index("tp") * heads_dev
    own_logit = lax.dynamic_slice_in_dim(part_logit, first_head, heads_dev, 1)
    own_bias = lax.dynamic_slice_in_dim(forget_bias, first_head, heads_dev, 0)
    fresh_gate = jax.nn.log_sigmoid(own_logit * rscale + own_bias)
    bias = fresh_gate[:, :, None] + (grand - lower - running)
    factor = HEAD_DIM ** (-0.5)
    keys = cache_keys.reshape(seqs, span, heads_dev, HEAD_DIM)
    values = cache_values.reshape(seqs, span, heads_dev, HEAD_DIM)
    scores = (
        jnp.einsum("bphd,bhd->bhp", keys, query, preferred_element_type=jnp.float32) * factor + bias
    )
    top = jnp.max(jnp.where(live, scores, FLOOR), axis=2)
    weights = jnp.where(live, jnp.exp(scores - top[:, :, None]), 0.0)
    mass = jnp.sum(weights, axis=2)
    summed = jnp.einsum(
        "bhp,bphd->bhd", weights.astype(jnp.bfloat16), values, preferred_element_type=jnp.float32
    )
    top, mass, summed = joined((top, mass, summed), "kv", join_parts)
    own = jnp.einsum("bhd,bhd->bh", query, fresh_key, preferred_element_type=jnp.float32) * factor
    peak = jnp.maximum(top, own)
    keep = jnp.exp(top - peak)
    fresh = jnp.exp(own - peak)
    attended = (
        (summed * keep[:, :, None] + fresh_value.astype(jnp.float32) * fresh[:, :, None])
        / (mass * keep + fresh)[:, :, None]
    ).astype(jnp.bfloat16)
    attended = attended.reshape(seqs, heads_dev * HEAD_DIM)
    return jnp.dot(attended, out_weight, preferred_element_type=jnp.float32)


def advance(shard, block, partial_value, weight):
    total = lax.psum(partial_value, "tp")
    return (shard, (block.astype(jnp.float32) + weight * total).astype(jnp.bfloat16))


def local(
    hidden_rows,
    first_gain,
    first_gate,
    first_up,
    first_down,
    mix_gain,
    query_weight,
    key_weight,
    value_weight,
    forget_weight,
    forget_bias,
    out_weight,
    second_gain,
    second_gate,
    second_up,
    second_down,
    cache_keys,
    cache_values,
    cache_gates,
    lengths,
):
    shard = hidden_rows
    block = widen(shard)
    partial_value = feed_forward(block, first_gain, first_gate, first_up, first_down)
    shard, block = advance(shard, block, partial_value, 0.5)
    partial_value = attention(
        block,
        mix_gain,
        query_weight,
        key_weight,
        value_weight,
        forget_weight,
        forget_bias,
        out_weight,
        cache_keys,
        cache_values,
        cache_gates,
        lengths,
    )
    shard, block = advance(shard, block, partial_value, 1.0)
    partial_value = feed_forward(block, second_gain, second_gate, second_up, second_down)
    shard, block = advance(shard, block, partial_value, 0.5)
    columns = hidden_rows.shape[1]
    return lax.dynamic_slice_in_dim(block, lax.axis_index("tp") * columns, columns, 1)


def solution(mesh):
    return jax.shard_map(
        local,
        mesh=mesh,
        in_specs=(
            P(None, ("kv", "tp")),
            P("kv"),
            P("kv", "tp"),
            P("kv", "tp"),
            P("tp", "kv"),
            P("kv"),
            P("kv", "tp"),
            P("kv", "tp"),
            P("kv", "tp"),
            P("kv", None),
            P(),
            P("tp", "kv"),
            P("kv"),
            P("kv", "tp"),
            P("kv", "tp"),
            P("tp", "kv"),
            P(None, "kv", "tp"),
            P(None, "kv", "tp"),
            P(None, "tp", "kv"),
            P(),
        ),
        out_specs=P(None, ("kv", "tp")),
        check_vma=False,
    )
```

profile of v0, /device:TPU:0, one launch (start us, length us, event | category | flops | bytes accessed | tf_op | source)
XLA Modules:
  0.0 400.4 jit_solution(7020302194779085242)
XLA Ops:
  6.5 6.5 %all_gather.27 = bf16[28,512]{1,0:T(8,128)(2,1)S(1)} all-gather(bf16[28,128]{1,0:T(8,128)(2,1)} %param.24), channel_id=1, replica_groups=mesh['kv'=8,'tp'=4] {'tp'}, dimensions={1}, use_global_device_ids=true | all-gather | bytes 35840 | tf_op jit(solution)/shard_map/all_gather | solution.py:34
  13.1 2.0 fusion.27
  16.8 2.3 reduce-window.6
  20.8 31.5 %all-gather = f32[224,4,1]{1,2,0:T(1,128)S(1)} all-gather(f32[28,4,1]{1,2,0:T(1,128)S(1)} %copy.78), channel_id=2, replica_groups=mesh['kv'=8,'tp'=4] {'kv'}, dimensions={0}, use_global_device_ids=true | all-gather | bytes 4032 | tf_op jit(solution)/shard_map/all_gather | solution.py:14
  52.6 21.3 %psum.106 = f32[28,1]{0,1:T(1,128)S(1)} all-reduce(f32[28,1]{0,1:T(1,128)S(1)} %bitcast.89), channel_id=1, replica_groups=mesh['kv'=8,'tp'=4] {'kv'}, use_global_device_ids=true, to_apply=%region_2.0 | all-reduce | flops 28 | bytes 224 | tf_op jit(solution)/shard_map/psum | solution.py:48
  73.9 19.2 %all-reduce.11.cloned.1.call-done = (f32[28,2816]{1,0:T(8,128)}, f32[28,2816]{1,0:T(8,128)}) async-done(((f32[28,2816]{1,0:T(8,128)}, f32[28,2816]{1,0:T(8,128)}), (f32[28,2816]{1,0:T(8,128)}, f32[28,2816]{1,0:T(8,128)})) %all-reduce.11.cloned.1.call-update) | async-done | bytes 630800 | tf_op jit(solution)/shard_map/psum | solution.py:48
  93.1 2.7 fusion.6
  95.8 10.7 %psum.108 = f32[28,512]{1,0:T(8,128)S(1)} all-reduce(f32[28,512]{1,0:T(8,128)S(1)} %fusion.6), channel_id=1, replica_groups=mesh['kv'=8,'tp'=4] {'tp'}, use_global_device_ids=true, to_apply=%region_4.5 | all-reduce | flops 14336 | bytes 114688 | tf_op jit(solution)/shard_map/psum | solution.py:133
  107.9 1.9 fusion.33
  109.8 1.9 fusion.31
  114.0 10.4 %copy.97 = bf16[28,256,512]{1,2,0:T(8,128)(2,1)} copy(bf16[28,256,512]{2,1,0:T(8,128)(2,1)} %param.40) | data formatting | bytes 14680064 | tf_op jit(solution)/shard_map/reshape | solution.py:108
  124.5 60.4 %all-reduce.7.cloned.1.call-done = (f32[28,512]{1,0:T(8,128)}, f32[28,1]{0,1:T(1,128)}, f32[28,512]{1,0:T(8,128)}, f32[28,4,1]{0,1,2:T(4,128)}, f32[28,16]{0,1:T(8,128)}, /*index=5*/f32[28,512]{1,0:T(8,128)}) async-done(((f32[28,512]{1,0:T(8,128)}, f32[28,1]{0,1:T(1,128)}, f32[28,512]{1,0:T(8,128)}, f32[28,4,1]{0,1,2:T(4,128)}, f32[28,16]{0,1:T(8,128)}, /*index=5*/f32[28,512]{1,0:T(8,128)}), ...) | async-done | bytes 174400 | tf_op jit(solution)/shard_map/psum | solution.py:95
  188.2 4.1 %fusion.54 = f32[28,4,1,256]{3,2,1,0:T(1,128)S(1)} fusion(bf16[28,4,128,1]{2,3,1,0:T(2,128)(2,1)S(1)} %reshape.110, bf16[28,256,4,128]{1,3,2,0:T(8,128)(2,1)} %bitcast.79), kind=kOutput, calls=%fused_computation.84 | convolution fusion | flops 7340032 | bytes 7483392 | tf_op jit(solution)/shard_map/bphd,bhd->bhp/dot_general | solution.py:111
  193.0 26.1 %all-gather.5 = f32[8,28,4]{1,2,0:T(4,128)S(1)} all-gather(f32[1,28,4]{1,2,0:T(4,128)S(1)} %bitcast.86), channel_id=4, replica_groups=mesh['kv'=8,'tp'=4] {'kv'}, dimensions={0}, use_global_device_ids=true | all-gather | bytes 4032 | tf_op jit(solution)/shard_map/all_gather | solution.py:26
  219.7 26.1 %all-gather.4 = f32[8,28,4]{1,2,0:T(4,128)S(1)} all-gather(f32[1,28,4]{1,2,0:T(4,128)S(1)} %bitcast.85), channel_id=3, replica_groups=mesh['kv'=8,'tp'=4] {'kv'}, dimensions={0}, use_global_device_ids=true | all-gather | bytes 4032 | tf_op jit(solution)/shard_map/all_gather | solution.py:26
  246.4 4.1 %fusion.3 = f32[28,4,1,128]{3,2,1,0:T(1,128)S(1)} fusion(bf16[28,4,256,1]{2,1,0,3:T(4,128)(2,1)S(1)} %get-tuple-element.207, bf16[28,256,512]{2,1,0:T(8,128)(2,1)} %param.41), kind=kOutput, calls=%fused_computation.10 | convolution fusion | flops 7340032 | bytes 7454720 | tf_op jit(solution)/shard_map/bhp,bphd->bhd/dot_general | solution.py:116
  250.6 31.3 %all-gather.3 = f32[224,4,128]{2,1,0:T(4,128)S(1)} all-gather(f32[28,4,128]{2,1,0:T(4,128)S(1)} %bitcast.84), channel_id=5, replica_groups=mesh['kv'=8,'tp'=4] {'kv'}, dimensions={0}, use_global_device_ids=true | all-gather | bytes 516096 | tf_op jit(solution)/shard_map/all_gather | solution.py:26
  282.2 7.9 %while.28 = (s32[]{:T(128)}, f32[28,4]{0,1:T(4,128)S(1)}, f32[28,4]{0,1:T(4,128)S(1)}, f32[28,4,128]{2,1,0:T(4,128)S(1)}, f32[7,28,4]{1,2,0:T(4,128)}, /*index=5...) while((s32[]{:T(128)}, f32[28,4]{0,1:T(4,128)S(1)}, f32[28,4]{0,1:T(4,128)S(1)}, ...), condition=%wide.region_17.18_spmd, body=%wide.region_16.17_spmd.sunk | while | flops 43682 | bytes 178405 | solution.py:29
  291.8 10.7 %psum.115 = f32[28,512]{1,0:T(8,128)S(1)} all-reduce(f32[28,512]{1,0:T(8,128)S(1)} %fusion.55), channel_id=1, replica_groups=mesh['kv'=8,'tp'=4] {'tp'}, use_global_device_ids=true, to_apply=%region_20.21 | all-reduce | flops 14336 | bytes 114688 | tf_op jit(solution)/shard_map/psum | solution.py:133
  302.6 3.3 fusion.40
  307.3 17.5 %psum.117 = f32[28,1]{0,1:T(1,128)S(1)} all-reduce(f32[28,1]{0,1:T(1,128)S(1)} %bitcast.88), channel_id=1, replica_groups=mesh['kv'=8,'tp'=4] {'kv'}, use_global_device_ids=true, to_apply=%region_23.24 | all-reduce | flops 28 | bytes 224 | tf_op jit(solution)/shard_map/psum | solution.py:48
  324.8 55.1 %all-reduce.9.cloned.1.call-done = (f32[28,2816]{1,0:T(8,128)}, f32[28,2816]{1,0:T(8,128)}) async-done(((f32[28,2816]{1,0:T(8,128)}, f32[28,2816]{1,0:T(8,128)}), (f32[28,2816]{1,0:T(8,128)}, f32[28,2816]{1,0:T(8,128)})) %all-reduce.9.cloned.1.call-update) | async-done | bytes 630800 | tf_op jit(solution)/shard_map/psum | solution.py:48
  379.9 2.7 fusion.7
  382.6 10.7 %psum.119 = f32[28,512]{1,0:T(8,128)S(1)} all-reduce(f32[28,512]{1,0:T(8,128)S(1)} %fusion.7), channel_id=1, replica_groups=mesh['kv'=8,'tp'=4] {'tp'}, use_global_device_ids=true, to_apply=%region_25.26 | all-reduce | flops 14336 | bytes 114688 | tf_op jit(solution)/shard_map/psum | solution.py:133
  (129 shorter events, 24.5 us)
Async XLA Ops:
  6.5 6.5 %copy-start = (bf16[512,2816]{1,0:T(8,128)(2,1)S(1)}, bf16[512,2816]{1,0:T(8,128)(2,1)}, u32[]{:S(2)}) copy-start(bf16[512,2816]{1,0:T(8,128)(2,1)} %param.27) | copy-start | bytes 8650756
  6.5 8.6 %copy-start.6 = (f32[512]{0:T(512)S(1)}, f32[512]{0:T(512)}, u32[]{:S(2)}) copy-start(f32[512]{0:T(512)} %param.25) | copy-start | bytes 6148
  6.5 86.6 %all-reduce.11.cloned.1.call-start = ((), (), s32[]{:S(2)}) async-start(), calls=%async_computation.2 | async-start | bytes 1441792 | tf_op jit(solution)/shard_map/psum | solution.py:48
  6.5 8.6 %copy-start.1 = (bf16[512,2816]{1,0:T(8,128)(2,1)S(1)}, bf16[512,2816]{1,0:T(8,128)(2,1)}, u32[]{:S(2)}) copy-start(bf16[512,2816]{1,0:T(8,128)(2,1)} %param.26) | copy-start | bytes 8650756
  13.1 3.5 copy-start.8
  13.1 3.6 copy-start.3
  16.5 168.4 %all-reduce.7.cloned.1.call-start = ((), (), s32[]{:S(2)}) async-start(), calls=%async_computation | async-start | bytes 414720 | tf_op jit(solution)/shard_map/psum | solution.py:95
  16.8 90.4 %copy-start.4 = (f32[512]{0:T(512)S(1)}, f32[512]{0:T(512)}, u32[]{:S(2)}) copy-start(f32[512]{0:T(512)} %param.29) | copy-start | bytes 6148
  16.8 90.4 %copy-start.5 = (bf16[512,16]{0,1:T(8,128)(2,1)S(1)}, bf16[512,16]{0,1:T(8,128)(2,1)}, u32[]{:S(2)}) copy-start(bf16[512,16]{0,1:T(8,128)(2,1)} %param.33) | copy-start | bytes 49156
  113.5 266.4 %all-reduce.9.cloned.1.call-start = ((), (), s32[]{:S(2)}) async-start(), calls=%async_computation.1 | async-start | bytes 1441792 | tf_op jit(solution)/shard_map/psum | solution.py:48
  114.0 10.4 %copy-start.9 = (f32[16]{0:T(128)S(1)}, f32[16]{0:T(128)}, u32[]{:S(2)}) copy-start(f32[16]{0:T(128)} %param.34) | copy-start | bytes 196
  250.6 52.1 %copy-start.7 = (f32[512]{0:T(512)S(1)}, f32[512]{0:T(512)}, u32[]{:S(2)}) copy-start(f32[512]{0:T(512)} %param.36) | copy-start | bytes 6148
  302.5 3.4 copy-start.2
Sparse Core Ops, SparseCore 0:
  16.6 76.4 all-reduce.10
  113.6 71.1 all-reduce.6
  307.4 72.4 all-reduce.8
where the time goes:
time: 401 us; the launch traced here: 400 us
  blocking collectives  192 us (48%)
  waiting for transfers between devices  135 us (34%)
  matrix products  29.2 us (7%)
  local copies, waits for them, and re-layouts  15.8 us (4%)
  other arithmetic  14.4 us (4%)
  between operations  13.4 us (3%)
    all_gather x3, blocking collectives, joined(): pieces = jax.tree.map(lambda part: lax.all_gather(part, axis), value)  83.5 us
    psum x2, waiting for transfers between devices, feed_forward(): gate, up_act, squares = lax.psum((gate, up_act, squares), 'kv')  74.3 us
    psum x1, waiting for transfers between devices, attention(): lax.psum((part_query, part_key, part_value, part_logit, squares, local_to...  60.4 us
    psum x2, blocking collectives, feed_forward(): gate, up_act, squares = lax.psum((gate, up_act, squares), 'kv')  38.8 us
    psum x3, blocking collectives, advance(): total = lax.psum(partial_value, 'tp')  32 us
    all_gather x1, blocking collectives, entering(): everything = lax.all_gather(x, axis)  31.5 us
    reshape x1, local copies, waits for them, and re-layouts, attention(): keys = cache_keys.reshape(seqs, span, heads_dev, HEAD_DIM)  10.4 us
  transfers between devices with their start and end apart: 3, of which 3 were waited for; matrix products, arithmetic and copies ran while one was open for 4% of the time, Pallas kernels for 0%

commit v1 on v0

--- a/solution.py
+++ b/solution.py
@@ -130,7 +130,7 @@
 
 
 def advance(shard, block, partial_value, weight):
-    total = lax.psum(partial_value, "tp")
+    total = jax.lax.all_gather(partial_value, axis_name="tp").sum(axis=0)
     return (shard, (block.astype(jnp.float32) + weight * total).astype(jnp.bfloat16))
 
 

time: 401 us -> 386 us (0.963)
  blocking collectives: 192 us -> 178 us
    psum x3 -> x0, blocking collectives: 32 us -> none  [advance(): total = lax.psum(partial_value, 'tp')]
    all_gather x0 -> x3, blocking collectives: none -> 17.3 us  [advance(): total = jax.lax.all_gather(partial_value, axis_name='tp').sum(axis=0)]
where the time goes in v1:
time: 386 us; the launch traced here: 385 us
  blocking collectives  178 us (46%)
  waiting for transfers between devices  134 us (35%)
  matrix products  29.2 us (8%)
  local copies, waits for them, and re-layouts  15.8 us (4%)
  other arithmetic  14.5 us (4%)
  between operations  13.4 us (3%)
    all_gather x3, blocking collectives, joined(): pieces = jax.tree.map(lambda part: lax.all_gather(part, axis), value)  83.5 us
    psum x2, waiting for transfers between devices, feed_forward(): gate, up_act, squares = lax.psum((gate, up_act, squares), 'kv')  73.8 us
    psum x1, waiting for transfers between devices, attention(): lax.psum((part_query, part_key, part_value, part_logit, squares, local_to...  60.1 us
    psum x2, blocking collectives, feed_forward(): gate, up_act, squares = lax.psum((gate, up_act, squares), 'kv')  39 us
    all_gather x1, blocking collectives, entering(): everything = lax.all_gather(x, axis)  31.5 us
    all_gather x3, blocking collectives, advance(): total = jax.lax.all_gather(partial_value, axis_name='tp').sum(axis=0)  17.3 us
    reshape x1, local copies, waits for them, and re-layouts, attention(): keys = cache_keys.reshape(seqs, span, heads_dev, HEAD_DIM)  10.4 us
  transfers between devices with their start and end apart: 3, of which 3 were waited for; matrix products, arithmetic and copies ran while one was open for 4% of the time, Pallas kernels for 0%

profile of v1, /device:TPU:0, one launch (start us, length us, event | category | flops | bytes accessed | tf_op | source)
XLA Modules:
  0.0 385.1 jit_solution(10716950421049110579)
XLA Ops:
  6.5 6.5 %all_gather.45 = bf16[28,512]{1,0:T(8,128)(2,1)S(1)} all-gather(bf16[28,128]{1,0:T(8,128)(2,1)} %param.24), channel_id=1, replica_groups=mesh['kv'=8,'tp'=4] {'tp'}, dimensions={1}, use_global_device_ids=true | all-gather | bytes 35840 | tf_op jit(solution)/shard_map/all_gather | solution.py:34
  13.1 2.0 fusion.25
  16.8 2.3 reduce-window.6
  20.8 31.5 %all-gather.1 = f32[224,4,1]{1,2,0:T(1,128)S(1)} all-gather(f32[28,4,1]{1,2,0:T(1,128)S(1)} %copy.78), channel_id=3, replica_groups=mesh['kv'=8,'tp'=4] {'kv'}, dimensions={0}, use_global_device_ids=true | all-gather | bytes 4032 | tf_op jit(solution)/shard_map/all_gather | solution.py:14
  52.6 21.3 %psum.85 = f32[28,1]{0,1:T(1,128)S(1)} all-reduce(f32[28,1]{0,1:T(1,128)S(1)} %bitcast.95), channel_id=1, replica_groups=mesh['kv'=8,'tp'=4] {'kv'}, use_global_device_ids=true, to_apply=%region_2.0 | all-reduce | flops 28 | bytes 224 | tf_op jit(solution)/shard_map/psum | solution.py:48
  73.9 19.2 %all-reduce.11.cloned.1.call-done = (f32[28,2816]{1,0:T(8,128)}, f32[28,2816]{1,0:T(8,128)}) async-done(((f32[28,2816]{1,0:T(8,128)}, f32[28,2816]{1,0:T(8,128)}), (f32[28,2816]{1,0:T(8,128)}, f32[28,2816]{1,0:T(8,128)})) %all-reduce.11.cloned.1.call-update) | async-done | bytes 630800 | tf_op jit(solution)/shard_map/psum | solution.py:48
  93.1 2.7 convolution_bitcast_fusion.1
  95.8 5.8 %all-gather.7 = f32[4,28,512]{2,1,0:T(8,128)S(1)} all-gather(f32[1,28,512]{2,1,0:T(8,128)S(1)} %convolution_bitcast_fusion.1), channel_id=2, replica_groups=mesh['kv'=8,'tp'=4] {'tp'}, dimensions={0}, use_global_device_ids=true | all-gather | bytes 286720 | tf_op jit(solution)/shard_map/all_gather | solution.py:133
  103.1 1.9 fusion.31
  104.9 1.9 fusion.29
  109.1 10.4 %copy.97 = bf16[28,256,512]{1,2,0:T(8,128)(2,1)} copy(bf16[28,256,512]{2,1,0:T(8,128)(2,1)} %param.40) | data formatting | bytes 14680064 | tf_op jit(solution)/shard_map/reshape | solution.py:108
  119.6 60.1 %all-reduce.7.cloned.1.call-done = (f32[28,512]{1,0:T(8,128)}, f32[28,1]{0,1:T(1,128)}, f32[28,512]{1,0:T(8,128)}, f32[28,4,1]{0,1,2:T(4,128)}, f32[28,16]{0,1:T(8,128)}, /*index=5*/f32[28,512]{1,0:T(8,128)}) async-done(((f32[28,512]{1,0:T(8,128)}, f32[28,1]{0,1:T(1,128)}, f32[28,512]{1,0:T(8,128)}, f32[28,4,1]{0,1,2:T(4,128)}, f32[28,16]{0,1:T(8,128)}, /*index=5*/f32[28,512]{1,0:T(8,128)}), ...) | async-done | bytes 174400 | tf_op jit(solution)/shard_map/psum | solution.py:95
  183.1 4.1 %fusion.52 = f32[28,4,1,256]{3,2,1,0:T(1,128)S(1)} fusion(bf16[28,4,128,1]{2,3,1,0:T(2,128)(2,1)S(1)} %reshape.122, bf16[28,256,4,128]{1,3,2,0:T(8,128)(2,1)} %bitcast.85), kind=kOutput, calls=%fused_computation.85 | convolution fusion | flops 7340032 | bytes 7483392 | tf_op jit(solution)/shard_map/bphd,bhd->bhp/dot_general | solution.py:111
  187.8 26.1 %all-gather.9 = f32[8,28,4]{1,2,0:T(4,128)S(1)} all-gather(f32[1,28,4]{1,2,0:T(4,128)S(1)} %bitcast.92), channel_id=5, replica_groups=mesh['kv'=8,'tp'=4] {'kv'}, dimensions={0}, use_global_device_ids=true | all-gather | bytes 4032 | tf_op jit(solution)/shard_map/all_gather | solution.py:26
  214.6 26.1 %all-gather.8 = f32[8,28,4]{1,2,0:T(4,128)S(1)} all-gather(f32[1,28,4]{1,2,0:T(4,128)S(1)} %bitcast.91), channel_id=4, replica_groups=mesh['kv'=8,'tp'=4] {'kv'}, dimensions={0}, use_global_device_ids=true | all-gather | bytes 4032 | tf_op jit(solution)/shard_map/all_gather | solution.py:26
  241.3 4.1 %fusion.3 = f32[28,4,1,128]{3,2,1,0:T(1,128)S(1)} fusion(bf16[28,4,256,1]{2,1,0,3:T(4,128)(2,1)S(1)} %get-tuple-element.207, bf16[28,256,512]{2,1,0:T(8,128)(2,1)} %param.41), kind=kOutput, calls=%fused_computation.10 | convolution fusion | flops 7340032 | bytes 7454720 | tf_op jit(solution)/shard_map/bhp,bphd->bhd/dot_general | solution.py:116
  245.4 31.3 %all-gather.4 = f32[224,4,128]{2,1,0:T(4,128)S(1)} all-gather(f32[28,4,128]{2,1,0:T(4,128)S(1)} %bitcast.90), channel_id=6, replica_groups=mesh['kv'=8,'tp'=4] {'kv'}, dimensions={0}, use_global_device_ids=true | all-gather | bytes 516096 | tf_op jit(solution)/shard_map/all_gather | solution.py:26
  277.0 7.9 %while.28 = (s32[]{:T(128)}, f32[28,4]{0,1:T(4,128)S(1)}, f32[28,4]{0,1:T(4,128)S(1)}, f32[28,4,128]{2,1,0:T(4,128)S(1)}, f32[7,28,4]{1,2,0:T(4,128)}, /*index=5...) while((s32[]{:T(128)}, f32[28,4]{0,1:T(4,128)S(1)}, f32[28,4]{0,1:T(4,128)S(1)}, ...), condition=%wide.region_17.18_spmd, body=%wide.region_16.17_spmd.sunk | while | flops 43682 | bytes 178405 | solution.py:29
  286.7 5.8 %all-gather.10 = f32[4,28,512]{2,1,0:T(8,128)S(1)} all-gather(f32[1,28,512]{2,1,0:T(8,128)S(1)} %convolution_bitcast_fusion.2), channel_id=7, replica_groups=mesh['kv'=8,'tp'=4] {'tp'}, dimensions={0}, use_global_device_ids=true | all-gather | bytes 286720 | tf_op jit(solution)/shard_map/all_gather | solution.py:133
  292.6 3.3 fusion.38
  297.3 17.7 %psum.94 = f32[28,1]{0,1:T(1,128)S(1)} all-reduce(f32[28,1]{0,1:T(1,128)S(1)} %bitcast.94), channel_id=1, replica_groups=mesh['kv'=8,'tp'=4] {'kv'}, use_global_device_ids=true, to_apply=%region_23.24 | all-reduce | flops 28 | bytes 224 | tf_op jit(solution)/shard_map/psum | solution.py:48
  314.9 54.6 %all-reduce.9.cloned.1.call-done = (f32[28,2816]{1,0:T(8,128)}, f32[28,2816]{1,0:T(8,128)}) async-done(((f32[28,2816]{1,0:T(8,128)}, f32[28,2816]{1,0:T(8,128)}), (f32[28,2816]{1,0:T(8,128)}, f32[28,2816]{1,0:T(8,128)})) %all-reduce.9.cloned.1.call-update) | async-done | bytes 630800 | tf_op jit(solution)/shard_map/psum | solution.py:48
  369.5 2.7 convolution_bitcast_fusion
  372.2 5.8 %all-gather.11 = f32[4,28,512]{2,1,0:T(8,128)S(1)} all-gather(f32[1,28,512]{2,1,0:T(8,128)S(1)} %convolution_bitcast_fusion), channel_id=8, replica_groups=mesh['kv'=8,'tp'=4] {'tp'}, dimensions={0}, use_global_device_ids=true | all-gather | bytes 286720 | tf_op jit(solution)/shard_map/all_gather | solution.py:133
  (132 shorter events, 24.6 us)
Async XLA Ops:
  6.5 6.5 %copy-start = (bf16[512,2816]{1,0:T(8,128)(2,1)S(1)}, bf16[512,2816]{1,0:T(8,128)(2,1)}, u32[]{:S(2)}) copy-start(bf16[512,2816]{1,0:T(8,128)(2,1)} %param.27) | copy-start | bytes 8650756
  6.5 8.6 %copy-start.6 = (f32[512]{0:T(512)S(1)}, f32[512]{0:T(512)}, u32[]{:S(2)}) copy-start(f32[512]{0:T(512)} %param.25) | copy-start | bytes 6148
  6.5 86.6 %all-reduce.11.cloned.1.call-start = ((), (), s32[]{:S(2)}) async-start(), calls=%async_computation.2 | async-start | bytes 1441792 | tf_op jit(solution)/shard_map/psum | solution.py:48
  6.5 8.6 %copy-start.1 = (bf16[512,2816]{1,0:T(8,128)(2,1)S(1)}, bf16[512,2816]{1,0:T(8,128)(2,1)}, u32[]{:S(2)}) copy-start(bf16[512,2816]{1,0:T(8,128)(2,1)} %param.26) | copy-start | bytes 8650756
  13.1 3.5 copy-start.8
  13.1 3.6 copy-start.3
  16.5 163.2 %all-reduce.7.cloned.1.call-start = ((), (), s32[]{:S(2)}) async-start(), calls=%async_computation | async-start | bytes 414720 | tf_op jit(solution)/shard_map/psum | solution.py:95
  19.4 83.0 %copy-start.4 = (f32[512]{0:T(512)S(1)}, f32[512]{0:T(512)}, u32[]{:S(2)}) copy-start(f32[512]{0:T(512)} %param.29) | copy-start | bytes 6148
  19.4 83.0 %copy-start.5 = (bf16[512,16]{0,1:T(8,128)(2,1)S(1)}, bf16[512,16]{0,1:T(8,128)(2,1)}, u32[]{:S(2)}) copy-start(bf16[512,16]{0,1:T(8,128)(2,1)} %param.33) | copy-start | bytes 49156
  108.6 260.9 %all-reduce.9.cloned.1.call-start = ((), (), s32[]{:S(2)}) async-start(), calls=%async_computation.1 | async-start | bytes 1441792 | tf_op jit(solution)/shard_map/psum | solution.py:48
  109.1 10.4 %copy-start.9 = (f32[16]{0:T(128)S(1)}, f32[16]{0:T(128)}, u32[]{:S(2)}) copy-start(f32[16]{0:T(128)} %param.34) | copy-start | bytes 196
  245.4 47.2 %copy-start.7 = (f32[512]{0:T(512)S(1)}, f32[512]{0:T(512)}, u32[]{:S(2)}) copy-start(f32[512]{0:T(512)} %param.36) | copy-start | bytes 6148
  292.5 3.4 copy-start.2
Sparse Core Ops, SparseCore 0:
  16.6 76.4 all-reduce.10
  108.8 70.9 all-reduce.6
  297.4 72.0 all-reduce.8
